TPU v7x, 32 devices: a whole 2x2x4 slice. The times are simulated.
32 devices in a mesh: sp: 8 (over z, x), tp: 4 (over y, core).
Axes of the slice: x: 2, y: 2, z: 4, core: 2. Of those that a mesh axis runs over, the one named last changes fastest.
Arguments:
- stream: bfloat16 [4096, 2048], P(('sp', 'tp')), may hold values from -6 to 6
- projected: bfloat16 [4096, 2048], P('sp', 'tp'), may hold values from -6 to 6
- segments: int32 [4096], P('sp'), may hold values from 0 to 3, never falling along the last dimension, each value on 1 to 1536 neighbouring positions
- group_weight: bfloat16 [4, 512, 512], replicated, may hold values from -0.25 to 0.25
- group_scale: float32 [2048], replicated, may hold values from 0.1 to 1.9
- out_weight: bfloat16 [2048, 2048], replicated, may hold values from -0.125 to 0.125
- ffn_gain: float32 [2048], replicated, may hold values from 0.1 to 1.9
- routes: int32 [4096, 4], P(('sp', 'tp')), may hold values from 0 to 31, all different within a row; in each aligned block of 128 rows (0 to 127, 128 to 255, ...) at most 24 rows name the same one
- route_weights: float32 [4096, 4], P(('sp', 'tp')), may hold values from 0.05 to 0.5
- expert_gate: bfloat16 [32, 2048, 1024], P(('sp', 'tp')), may hold values from -0.25 to 0.25
- expert_up: bfloat16 [32, 2048, 1024], P(('sp', 'tp')), may hold values from -0.25 to 0.25
- expert_down: bfloat16 [32, 1024, 2048], P(('sp', 'tp')), may hold values from -0.1875 to 0.1875
Outputs:
- combined: bfloat16 [4096, 2048], P(('sp', 'tp'))
Inputs may be any that keep to these rules, and one draw needn't show every extreme that they name: `segments`: document numbers never fall along the positions; a document has 1 to 1536 positions, and one has exactly 1536. `routes`: each row names 4 different experts. Among the 128 rows of one device (aligned blocks), no expert is named more than 24 times, and in some blocks one is named exactly 24 times.
All inputs are finite; a program needn't handle non-finite values.
Results may differ from a plain program's by a relative error of at most 0.015.
Values may be sent and summed in bfloat16 or wider, within the bound.
A program may use at most 128 MiB of HBM per device.

v0:
```python
import jax
import jax.numpy as jnp
from jax import lax
from jax.sharding import PartitionSpec as P

GROUPS = 4


norm_eps = 1e-05
clamp_limit = 7.0
sigmoid_alpha = 1.702
longest_window = 16


def carried_in(value, axis, join, neutral):
    count, mine = (lax.axis_size(axis), lax.axis_index(axis))
    pieces = jax.tree.map(lambda part: lax.all_gather(part, axis), value)
    so_far = jax.tree.map(
        lambda part, zero: jnp.full_like(part, 0) + jnp.asarray(zero, part.dtype), value, neutral
    )

    def hop(position, so_far):
        longer = join(so_far, jax.tree.map(lambda part: part[position], pieces))
        return jax.tree.map(lambda new, old: jnp.where(position < mine, new, old), longer, so_far)

    return lax.fori_loop(0, count - 1, hop, so_far)


def rms_scale(resid, gain):
    values = resid.astype(jnp.float32)
    inverse = lax.rsqrt(jnp.mean(values * values, -1, keepdims=True) + norm_eps)
    return (values * inverse * gain).astype(jnp.bfloat16)


def run_expert(block, gate_matrix, up_matrix, down_matrix):
    leading = block.shape[:-1]
    flat_rows = block.reshape(-1, block.shape[-1])
    gate_value = jnp.dot(flat_rows, gate_matrix, preferred_element_type=jnp.float32)
    up_value = jnp.dot(flat_rows, up_matrix, preferred_element_type=jnp.float32)
    gated = jnp.minimum(gate_value, clamp_limit)
    linear = jnp.clip(up_value, -clamp_limit, clamp_limit)
    activated = (gated * jax.nn.sigmoid(sigmoid_alpha * gated) * (linear + 1.0)).astype(
        jnp.bfloat16
    )
    result = jnp.dot(activated, down_matrix, preferred_element_type=jnp.float32).astype(
        jnp.bfloat16
    )
    return result.reshape(leading + (down_matrix.shape[1],))


def keep_latter(earlier, latter):
    present = latter[1] >= 0
    return (
        jnp.where(present[..., None], latter[0], earlier[0]),
        jnp.where(present, latter[1], earlier[1]),
    )


def body(
    stream,
    projected,
    segments,
    group_weight,
    group_scale,
    out_weight,
    ffn_gain,
    routes,
    route_weights,
    expert_gate,
    expert_up,
    expert_down,
):
    row_count, channels = projected.shape
    tp_count = lax.axis_size("tp")
    sp_count = lax.axis_size("sp")
    model_width = channels * tp_count
    group_width = model_width // GROUPS
    rim_rows = longest_window - 1
    channel = lax.axis_index("tp") * channels + jnp.arange(channels, dtype=jnp.int32)
    window = jnp.left_shift(jnp.full((channels,), 2, jnp.int32), channel // group_width)
    identity = (jnp.zeros((rim_rows, channels), jnp.bfloat16), jnp.full((rim_rows,), -1, jnp.int32))
    before_rows, before_docs = carried_in(
        (projected[row_count - rim_rows :], segments[row_count - rim_rows :]),
        "sp",
        keep_latter,
        identity,
    )
    extended = jnp.concatenate([before_rows, projected], 0)
    extended_docs = jnp.concatenate([before_docs, segments], 0)
    window_sum = jnp.zeros((row_count, channels), jnp.float32)
    window_count = jnp.zeros((row_count, channels), jnp.float32)
    for offset in range(longest_window):
        earlier_rows = extended[rim_rows - offset : rim_rows - offset + row_count].astype(
            jnp.float32
        )
        earlier_docs = extended_docs[rim_rows - offset : rim_rows - offset + row_count]
        included = (earlier_docs == segments)[:, None] & (offset < window)[None, :]
        window_sum = window_sum + jnp.where(included, earlier_rows, jnp.float32(0.0))
        window_count = window_count + included.astype(jnp.float32)
    mixed = (window_sum / window_count - projected.astype(jnp.float32)).astype(jnp.bfloat16)
    tokens_here = lax.all_to_all(mixed, "tp", split_axis=0, concat_axis=1, tiled=True)
    tok_count = tokens_here.shape[0]
    grouped = jnp.einsum(
        "rgc,gcd->rgd",
        tokens_here.reshape(tok_count, GROUPS, group_width),
        group_weight,
        preferred_element_type=jnp.float32,
    ).reshape(tok_count, model_width)
    scaled = (grouped * group_scale).astype(jnp.bfloat16)
    mixer_out = jnp.dot(scaled, out_weight, preferred_element_type=jnp.float32)
    resid = (stream.astype(jnp.float32) + mixer_out).astype(jnp.bfloat16)
    normed = rms_scale(resid, ffn_gain)
    top_count = routes.shape[1]
    expert_count = sp_count * tp_count
    capacity = 3 * tok_count * top_count // (2 * expert_count)
    flat_routes = routes.reshape(-1)
    onehot = (flat_routes[:, None] == jnp.arange(expert_count, dtype=jnp.int32)[None, :]).astype(
        jnp.int32
    )
    ranking = jnp.sum((jnp.cumsum(onehot, 0) - onehot) * onehot, 1)
    slot_index = flat_routes * capacity + ranking
    token_of = jnp.arange(flat_routes.shape[0], dtype=jnp.int32) // top_count
    slot_token = jnp.zeros((expert_count * capacity,), jnp.int32).at[slot_index].set(token_of)
    slot_live = jnp.zeros((expert_count * capacity,), jnp.bool_).at[slot_index].set(True)
    outgoing = jnp.where(slot_live[:, None], normed[slot_token], jnp.zeros((), jnp.bfloat16))
    results = run_expert(
        lax.all_to_all(
            outgoing.reshape(expert_count, capacity, model_width),
            ("sp", "tp"),
            split_axis=0,
            concat_axis=0,
            tiled=True,
        ),
        expert_gate[0],
        expert_up[0],
        expert_down[0],
    )
    returned = lax.all_to_all(results, ("sp", "tp"), split_axis=0, concat_axis=0, tiled=True)
    picked = returned.reshape(expert_count * capacity, model_width)[slot_index]
    weighted = picked.astype(jnp.float32) * route_weights.reshape(-1)[:, None]
    moe_sum = jnp.sum(weighted.reshape(tok_count, top_count, model_width), 1)
    return (resid.astype(jnp.float32) + moe_sum).astype(jnp.bfloat16)


def solution(mesh):
    in_specs = (
        P(("sp", "tp"), None),
        P("sp", "tp"),
        P("sp"),
        P(),
        P(),
        P(),
        P(),
        P(("sp", "tp"), None),
        P(("sp", "tp"), None),
        P(("sp", "tp"), None, None),
        P(("sp", "tp"), None, None),
        P(("sp", "tp"), None, None),
    )
    out_specs = P(("sp", "tp"), None)
    return jax.shard_map(body, mesh=mesh, in_specs=in_specs, out_specs=out_specs, check_vma=False)
```

profile of v0, /device:TPU:0, one launch (start us, length us, event | category | flops | bytes accessed | tf_op | source)
XLA Modules:
  0.0 276.2 jit_solution(8071681615724556386)
XLA Ops:
  0.2 1.4 dynamic-slice
  2.3 0.8 slice_dynamic-update-slice_fusion
  3.2 13.1 %all-reduce = s32[120]{0:T(128)S(1)} all-reduce(s32[120]{0:T(128)S(1)} %slice_dynamic-update-slice_fusion), channel_id=2, replica_groups=mesh['sp'=8,'tp'=4] {'sp'}, use_global_device_ids=true, to_apply=%add | all-reduce | flops 120 | bytes 960
  16.2 0.1 reshape.217
  16.3 0.7 slice_bitcast_fusion
  17.1 30.5 %all-gather.2 = bf16[8,15,512]{2,1,0:T(8,128)(2,1)S(1)} all-gather(bf16[1,15,512]{2,1,0:T(8,128)(2,1)S(1)} %slice_bitcast_fusion), channel_id=3, replica_groups=mesh['sp'=8,'tp'=4] {'sp'}, dimensions={0}, use_global_device_ids=true | all-gather | bytes 138240 | tf_op jit(solution)/shard_map/all_gather | solution.py:17
  47.6 0.9 while.16
  47.7 0.1 select_select_fusion.2
  47.8 0.1 select_select_fusion.2
  48.0 0.1 select_select_fusion.2
  48.1 0.1 select_select_fusion.2
  48.4 0.1 select_select_fusion.2
  48.5 0.8 pad_add_fusion
  49.2 0.8 slice_compare_fusion.14
  50.0 15.9 %fusion.45 = bf16[512,512]{1,0:T(8,128)(2,1)} fusion(bf16[512,512]{1,0:T(8,128)(2,1)} %param.15, bf16[15,512]{1,0:T(8,128)(2,1)S(1)} %get-tuple-element.116, f32[512]{0:T(512)S(1)} %get-tuple-element.183, pred[512]{0:T(512)(128)(4,1)S(1)} %get-tuple-element.167, pred[512]{0:T(512)(128)(4,1)S(1)} %get-tuple-element.168, ...), kind=kLoop, calls=%fused_computation.105 | loop fusion | flops 36700160 | bytes 1081856 | tf_op jit(solution)/shard_map/convert_element_type | solution.py:100
  65.9 4.1 %all-to-all-start = ((bf16[4,128,512]{2,1,0:T(8,128)(2,1)}), bf16[4,128,512]{2,1,0:T(8,128)(2,1)}, u32[]{:S(2)}, u32[]{:S(2)}) async-start(bf16[4,128,512]{2,1,0:T(8,128)(2,1)} %bitcast.2), calls=%async_computation | async-start | bytes 1048576 | tf_op jit(solution)/shard_map/all_to_all | solution.py:101
  70.0 0.8 copy.22
  70.8 0.1 eq.89
  70.9 0.1 eq.85
  71.0 0.7 broadcast_multiply_fusion
  71.7 1.2 reduce-window.6
  72.9 0.2 slice_reduce_fusion
  73.2 0.1 copy.21
  73.3 0.1 mul.75
  73.4 0.1 fusion.63
  73.5 2.4 scatter_custom_fusion.1
  76.0 2.4 scatter_custom_fusion
  78.4 0.1 broadcast_in_dim.109
  78.6 0.3 all-to-all-done
  78.9 1.5 convolution_bitcast_fusion
  80.4 1.3 copy.20
  81.7 1.6 fusion.44
  83.3 4.8 %multiply_reduce_fusion.1 = (f32[128]{0:T(128)S(1)}, f32[128,2048]{1,0:T(8,128)S(1)}) fusion(bf16[128,2048]{0,1:T(8,128)(2,1)S(1)} %fusion.44, bf16[2048,2048]{1,0:T(8,128)(2,1)} %param.19, bf16[128,2048]{1,0:T(8,128)(2,1)} %param.14), kind=kOutput, calls=%fused_computation.104 | convolution fusion | flops 1075314560 | bytes 10486272 | tf_op jit(solution)/shard_map/dot_general | solution.py:110
  88.1 1.0 copy-done.1
  89.1 0.2 multiply_convert_fusion.1
  89.3 4.3 %gather_fusion = bf16[768,2048]{1,0:T(8,128)(2,1)} fusion(bf16[128,2048]{1,0:T(8,128)(2,1)S(1)} %multiply_convert_fusion.1, s32[1024]{0:T(1024)S(1)} %pad_clamp_fusion.1), kind=kCustom, calls=%fused_computation | custom fusion | bytes 6294528 | tf_op jit(solution)/shard_map/gather | solution.py:125
  93.5 2.2 broadcast_select_fusion.2
  95.7 73.9 %all_to_all.26 = bf16[32,24,2048]{2,1,0:T(8,128)(2,1)S(1)} all-to-all(bf16[32,24,2048]{2,1,0:T(8,128)(2,1)S(1)} %broadcast_select_fusion.2), channel_id=1, replica_groups=mesh['sp'=8,'tp'=4] {'sp','tp'}, dimensions={0} | all-to-all | bytes 6291456 | tf_op jit(solution)/shard_map/all_to_all | solution.py:127
  169.6 3.4 %fusion.2 = f32[768,1024]{1,0:T(8,128)S(1)} fusion(bf16[768,2048]{1,0:T(8,128)(2,1)S(1)} %bitcast.72, bf16[1,2048,1024]{2,1,0:T(8,128)(2,1)S(1)} %copy-done.6), kind=kOutput, calls=%fused_computation.11 | convolution fusion | flops 3221225472 | bytes 10485760 | tf_op jit(solution)/shard_map/dot_general | solution.py:39
  173.1 4.1 %multiply_convert_fusion = bf16[768,1024]{1,0:T(8,128)(2,1)S(1)} fusion(f32[768,1024]{1,0:T(8,128)S(1)} %fusion.2, bf16[768,2048]{1,0:T(8,128)(2,1)S(1)} %bitcast.73, bf16[1,2048,1024]{2,1,0:T(8,128)(2,1)S(1)} %copy-done.7), kind=kOutput, calls=%fused_computation.17 | convolution fusion | flops 3229089792 | bytes 12058624 | tf_op jit(solution)/shard_map/dot_general | solution.py:38
  177.3 4.8 %fusion.6 = bf16[768,2048]{1,0:T(8,128)(2,1)} fusion(bf16[768,1024]{1,0:T(8,128)(2,1)S(1)} %multiply_convert_fusion, bf16[1,1024,2048]{2,1,0:T(8,128)(2,1)S(1)} %copy-done.8), kind=kOutput, calls=%fused_computation.16 | convolution fusion | flops 3222798336 | bytes 8912896 | tf_op jit(solution)/shard_map/dot_general | solution.py:45
  182.1 4.0 %all-to-all-start.2 = ((bf16[32,24,2048]{2,1,0:T(8,128)(2,1)}), bf16[32,24,2048]{2,1,0:T(8,128)(2,1)}, u32[]{:S(2)}, u32[]{:S(2)}) async-start(bf16[32,24,2048]{2,1,0:T(8,128)(2,1)} %bitcast.71), calls=%async_computation.2 | async-start | bytes 6291456 | tf_op jit(solution)/shard_map/all_to_all | solution.py:138
  186.1 0.1 copy.25
  186.2 71.2 %all-to-all-done.2 = bf16[32,24,2048]{2,1,0:T(8,128)(2,1)} async-done(((bf16[32,24,2048]{2,1,0:T(8,128)(2,1)}), bf16[32,24,2048]{2,1,0:T(8,128)(2,1)}, u32[]{:S(2)}, u32[]{:S(2)}) %all-to-all-start.2) | async-done | bytes 3145760 | tf_op jit(solution)/shard_map/all_to_all | solution.py:138
  257.5 7.6 %gather_fusion.1 = bf16[512,2048]{1,0:T(8,128)(2,1)} fusion(bf16[768,2048]{1,0:T(8,128)(2,1)} %bitcast.15, s32[1024]{0:T(1024)S(1)} %pad_clamp_fusion), kind=kCustom, calls=%fused_computation.1 | custom fusion | bytes 4196352 | tf_op jit(solution)/shard_map/gather | solution.py:139
  265.1 4.8 %reshape.184 = f32[128,4,2048]{2,1,0:T(4,128)} reshape(bf16[512,2048]{1,0:T(8,128)(2,1)} %gather_fusion.1) | data formatting | bytes 6291456 | tf_op jit(solution)/shard_map/convert_element_type | solution.py:140
  269.8 5.5 %multiply_reduce_fusion = f32[128,2048]{1,0:T(8,128)S(1)} fusion(f32[128,4,2048]{2,1,0:T(4,128)} %reshape.184, f32[128,4]{1,0:T(8,128)S(1)} %copy.25), kind=kLoop, calls=%fused_computation.15 | loop fusion | flops 1835008 | bytes 5244928 | tf_op jit(solution)/shard_map/reduce_sum | solution.py:141
  275.3 0.9 add_convert_fusion
  (54 shorter events, 0.6 us)
Async XLA Ops:
  0.0 78.9 %copy-start = (bf16[4,512,512]{2,1,0:T(8,128)(2,1)S(1)}, bf16[4,512,512]{2,1,0:T(8,128)(2,1)}, u32[]{:S(2)}) copy-start(bf16[4,512,512]{2,1,0:T(8,128)(2,1)} %param.17) | copy-start | bytes 6291460
  65.9 13.0 %all-to-all-start = ((bf16[4,128,512]{2,1,0:T(8,128)(2,1)}), bf16[4,128,512]{2,1,0:T(8,128)(2,1)}, u32[]{:S(2)}, u32[]{:S(2)}) async-start(bf16[4,128,512]{2,1,0:T(8,128)(2,1)} %bitcast.2), calls=%async_computation | async-start | bytes 1048576 | tf_op jit(solution)/shard_map/all_to_all | solution.py:101
  71.7 10.0 %copy-start.3 = (f32[2048]{0:T(1024)S(1)}, f32[2048]{0:T(1024)}, u32[]{:S(2)}) copy-start(f32[2048]{0:T(1024)} %param.18) | copy-start | bytes 24580
  83.3 5.8 %copy-start.4 = (f32[2048]{0:T(1024)S(1)}, f32[2048]{0:T(1024)}, u32[]{:S(2)}) copy-start(f32[2048]{0:T(1024)} %param.20) | copy-start | bytes 24580
  88.1 1.0 copy-start.1
  95.7 73.9 %copy-start.6 = (bf16[1,2048,1024]{2,1,0:T(8,128)(2,1)S(1)}, bf16[1,2048,1024]{2,1,0:T(8,128)(2,1)}, u32[]{:S(2)}) copy-start(bf16[1,2048,1024]{2,1,0:T(8,128)(2,1)} %param.24) | copy-start | bytes 12582916
  169.6 3.5 %copy-start.7 = (bf16[1,2048,1024]{2,1,0:T(8,128)(2,1)S(1)}, bf16[1,2048,1024]{2,1,0:T(8,128)(2,1)}, u32[]{:S(2)}) copy-start(bf16[1,2048,1024]{2,1,0:T(8,128)(2,1)} %param.23) | copy-start | bytes 12582916
  173.1 4.2 %copy-start.8 = (bf16[1,1024,2048]{2,1,0:T(8,128)(2,1)S(1)}, bf16[1,1024,2048]{2,1,0:T(8,128)(2,1)}, u32[]{:S(2)}) copy-start(bf16[1,1024,2048]{2,1,0:T(8,128)(2,1)} %param.25) | copy-start | bytes 12582916
  182.1 4.0 %copy-start.5 = (f32[128,4]{0,1:T(4,128)S(1)}, f32[128,4]{0,1:T(4,128)}, u32[]{:S(2)}) copy-start(f32[128,4]{0,1:T(4,128)} %param.22) | copy-start | bytes 6148
  182.1 75.4 %all-to-all-start.2 = ((bf16[32,24,2048]{2,1,0:T(8,128)(2,1)}), bf16[32,24,2048]{2,1,0:T(8,128)(2,1)}, u32[]{:S(2)}, u32[]{:S(2)}) async-start(bf16[32,24,2048]{2,1,0:T(8,128)(2,1)} %bitcast.71), calls=%async_computation.2 | async-start | bytes 6291456 | tf_op jit(solution)/shard_map/all_to_all | solution.py:138
  269.8 5.5 %copy-start.2 = (f32[128,2048]{1,0:T(8,128)S(1)}, f32[128,2048]{1,0:T(8,128)}, u32[]{:S(2)}) copy-start(f32[128,2048]{1,0:T(8,128)} %copy-done.1) | copy-start | bytes 3145732
where the time goes:
time: 278 us; the launch traced here: 276 us
  blocking collectives  117 us (42%)
  waiting for transfers between devices  71.6 us (26%)
  other arithmetic  30.6 us (11%)
  local copies, waits for them, and re-layouts  28.6 us (10%)
  matrix products  18.7 us (7%)
  starting transfers between devices  8.13 us (3%)
    all_to_all x1, blocking collectives, body(): lax.all_to_all(outgoing.reshape(expert_count, capacity, model_width), ('s...  73.9 us
    all_to_all x1, waiting for transfers between devices, body(): lax.all_to_all(results, ('sp', 'tp'), split_axis=0, concat_axis=0, tiled=...  71.2 us
    all_gather x1, blocking collectives, carried_in(): pieces = jax.tree.map(lambda part: lax.all_gather(part, axis), value)  30.5 us
    convert_element_type x1, other arithmetic, body(): (window_sum / window_count - projected.astype(jnp.float32)).astype(jnp.bf...  15.9 us
    unnamed x1, blocking collectives  13.1 us
    gather x1, local copies, waits for them, and re-layouts, body(): picked = returned.reshape(expert_count * capacity, model_width)[slot_index]  7.56 us
  transfers between devices with their start and end apart: 2, of which 2 were waited for; matrix products, arithmetic and copies ran while one was open for 3% of the time, Pallas kernels for 0%

commit v1 on v0

v1 whole, which is shorter than its diff:
```python
import jax
import jax.numpy as jnp
from jax import lax
from jax.experimental import pallas as pl
from jax.experimental.pallas import tpu as pltpu
from jax.sharding import PartitionSpec as P

GROUPS = 4


norm_eps = 1e-05
clamp_limit = 7.0
sigmoid_alpha = 1.702
longest_window = 16


def pool_kernel(group_width, halo_ref, rows_ref, docs_ref, mixed_ref):
    channels = rows_ref.shape[1]
    first = lax.axis_index("tp") * channels
    docs = docs_ref[...]
    same = [docs == pltpu.roll(docs, 1 << k, 0) for k in range(GROUPS)]
    for lane in range(0, channels, 128):
        cols = slice(lane, lane + 128)
        values = jnp.concatenate([halo_ref[:, cols], rows_ref[:, cols]], 0).astype(jnp.float32)
        total, count = values, jnp.ones_like(values)
        channel = first + lane + lax.broadcasted_iota(jnp.int32, values.shape, 1)
        for k in range(GROUPS):
            joins = same[k] & (channel >= k * group_width)
            total = jnp.where(joins, total + pltpu.roll(total, 1 << k, 0), total)
            count = jnp.where(joins, count + pltpu.roll(count, 1 << k, 0), count)
        mixed_ref[:, cols] = (total / count - values)[longest_window:].astype(jnp.bfloat16)


def pool(projected, segments, group_width):
    sp_count = lax.axis_size("sp")
    row_count, channels = projected.shape
    onward = [(i, i + 1) for i in range(sp_count - 1)]
    halo = lax.ppermute(projected[row_count - longest_window :], "sp", onward)
    halo_docs = lax.ppermute(segments[row_count - longest_window :], "sp", onward)
    halo_docs = jnp.where(lax.axis_index("sp") == 0, -1, halo_docs)
    docs = jnp.concatenate([halo_docs, segments])
    docs = jnp.broadcast_to(docs[:, None], (row_count + longest_window, 128))
    return pl.pallas_call(
        lambda *refs: pool_kernel(group_width, *refs),
        out_shape=jax.ShapeDtypeStruct((row_count, channels), jnp.bfloat16),
        name="pool",
    )(halo, projected, docs)


def slots_of(routes, expert_count, capacity):
    tok_count = routes.shape[0]
    named = routes[:, :, None] == jnp.arange(expert_count, dtype=jnp.int32)
    marks = jnp.sum(named.astype(jnp.float32), 1).astype(jnp.bfloat16)
    at = jnp.arange(tok_count, dtype=jnp.int32)
    earlier = (at[None, :] < at[:, None]).astype(jnp.bfloat16)
    before = jnp.dot(earlier, marks, preferred_element_type=jnp.float32)
    rank = jnp.sum(jnp.where(named, before[:, None, :], 0.0), 2).astype(jnp.int32)
    return routes * capacity + rank


def rms_scale(resid, gain):
    values = resid.astype(jnp.float32)
    inverse = lax.rsqrt(jnp.mean(values * values, -1, keepdims=True) + norm_eps)
    return (values * inverse * gain).astype(jnp.bfloat16)


def mixer(mixed, stream, group_weight, group_scale, out_weight, ffn_gain):
    tokens_here = lax.all_to_all(mixed, "tp", split_axis=0, concat_axis=1, tiled=True)
    group_width = group_weight.shape[1]
    grouped = jnp.concatenate(
        [
            jnp.dot(
                tokens_here[:, g * group_width : (g + 1) * group_width],
                group_weight[g],
                preferred_element_type=jnp.float32,
            )
            for g in range(GROUPS)
        ],
        1,
    )
    scaled = (grouped * group_scale).astype(jnp.bfloat16)
    mixer_out = jnp.dot(scaled, out_weight, preferred_element_type=jnp.float32)
    resid = (stream.astype(jnp.float32) + mixer_out).astype(jnp.bfloat16)
    return resid, rms_scale(resid, ffn_gain)


def run_expert(rows, gate_matrix, up_matrix, down_matrix):
    gate_value = jnp.dot(rows, gate_matrix, preferred_element_type=jnp.float32)
    up_value = jnp.dot(rows, up_matrix, preferred_element_type=jnp.float32)
    gated = jnp.minimum(gate_value, clamp_limit)
    linear = jnp.clip(up_value, -clamp_limit, clamp_limit)
    activated = (gated * jax.nn.sigmoid(sigmoid_alpha * gated) * (linear + 1.0)).astype(
        jnp.bfloat16
    )
    return jnp.dot(activated, down_matrix, preferred_element_type=jnp.float32).astype(jnp.bfloat16)


def body(
    stream,
    projected,
    segments,
    group_weight,
    group_scale,
    out_weight,
    ffn_gain,
    routes,
    route_weights,
    expert_gate,
    expert_up,
    expert_down,
):
    tok_count, model_width = stream.shape
    expert_count = lax.axis_size("sp") * lax.axis_size("tp")
    top_count = routes.shape[1]
    capacity = 3 * tok_count * top_count // (2 * expert_count)
    mixed = pool(projected, segments, group_weight.shape[1])
    slots = slots_of(routes, expert_count, capacity)
    resid, normed = mixer(mixed, stream, group_weight, group_scale, out_weight, ffn_gain)
    slot_ids = jnp.arange(expert_count * capacity, dtype=jnp.int32)
    chosen = slots[:, :, None] == slot_ids
    select = jnp.any(chosen, 1).astype(jnp.bfloat16)
    weigh = jnp.sum(jnp.where(chosen, route_weights[:, :, None], 0.0), 1).astype(jnp.bfloat16)
    outgoing = lax.dot_general(
        select, normed, (((0,), (0,)), ((), ())), preferred_element_type=jnp.float32
    ).astype(jnp.bfloat16)

    def exchange(rows):
        return lax.all_to_all(
            rows.reshape(expert_count, capacity, model_width),
            ("sp", "tp"),
            split_axis=0,
            concat_axis=0,
            tiled=True,
        ).reshape(expert_count * capacity, model_width)

    results = run_expert(exchange(outgoing), expert_gate[0], expert_up[0], expert_down[0])
    moe_sum = jnp.dot(weigh, exchange(results), preferred_element_type=jnp.float32)
    return (resid.astype(jnp.float32) + moe_sum).astype(jnp.bfloat16)


def solution(mesh):
    in_specs = (
        P(("sp", "tp"), None),
        P("sp", "tp"),
        P("sp"),
        P(),
        P(),
        P(),
        P(),
        P(("sp", "tp"), None),
        P(("sp", "tp"), None),
        P(("sp", "tp"), None, None),
        P(("sp", "tp"), None, None),
        P(("sp", "tp"), None, None),
    )
    out_specs = P(("sp", "tp"), None)
    return jax.shard_map(body, mesh=mesh, in_specs=in_specs, out_specs=out_specs, check_vma=False)
```

time: 278 us -> 204 us (0.73)
  blocking collectives: 117 us -> 76.4 us
  other arithmetic: 30.6 us -> 2 us
  local copies, waits for them, and re-layouts: 28.6 us -> 4.59 us
  waiting for transfers between devices: 71.6 us -> 79.8 us
  starting transfers between devices: 8.13 us -> 15.4 us
  matrix products: 18.7 us -> 22 us
  Pallas kernels: 0 us -> 3.25 us
    all_gather x1 -> x0, blocking collectives: 30.5 us -> none  [carried_in(): pieces = jax.tree.map(lambda part: lax.all_gather(part, axis), value)]
    convert_element_type x5 -> x0, other arithmetic: 18.5 us -> none  [the longest x1 15.9 us: body(): (window_sum / window_count - projected.astype(jnp.float32)).astype(jnp.bf...]
    unnamed x1 -> x0, blocking collectives: 13.1 us -> none
    gather x2 -> x0, local copies, waits for them, and re-layouts: 11.8 us -> none  [the longest x1 7.56 us: body(): picked = returned.reshape(expert_count * capacity, model_width)[slot_index]]
    ppermute x0 -> x2, starting transfers between devices: none -> 8.3 us  [the longest x1 4.86 us: pool(): lax.ppermute(segments[row_count - longest_window:], 'sp', onward)]
    all_to_all x2, waiting for transfers between devices: 71.6 us -> 79.8 us  [the longest x1 71.4 us: exchange(): lax.all_to_all(rows.reshape(expert_count, capacity, model_width), ('sp',...]
    unnamed x24 -> x22, local copies, waits for them, and re-layouts: 4.95 us -> 0.05 us
    scatter x2 -> x0, local copies, waits for them, and re-layouts: 4.89 us -> none  [the longest x1 2.45 us: body(): jnp.zeros((expert_count * capacity,), jnp.bool_).at[slot_index].set(True)]
  transfers between devices with their start and end apart: 2 -> 4, of which waited for: 2 -> 2; matrix products, arithmetic and copies ran while one was open for 3% -> 1% of each run, Pallas kernels for 0% -> 0%
where the time goes in v1:
time: 204 us
  waiting for transfers between devices  79.8 us (39%)
  blocking collectives  76.4 us (37%)
  matrix products  22 us (11%)
  starting transfers between devices  15.4 us (8%)
  local copies, waits for them, and re-layouts  4.59 us (2%)
  Pallas kernels  3.25 us (2%)
    all_to_all x1, blocking collectives, exchange(): lax.all_to_all(rows.reshape(expert_count, capacity, model_width), ('sp',...  76.4 us
    all_to_all x1, waiting for transfers between devices, exchange(): lax.all_to_all(rows.reshape(expert_count, capacity, model_width), ('sp',...  71.4 us
    all_to_all x1, waiting for transfers between devices, mixer(): lax.all_to_all(mixed, 'tp', split_axis=0, concat_axis=1, tiled=True)  8.45 us
    ppermute x1, starting transfers between devices, pool(): lax.ppermute(segments[row_count - longest_window:], 'sp', onward)  4.86 us
    dot_general x1, matrix products, mixer(): mixer_out = jnp.dot(scaled, out_weight, preferred_element_type=jnp.float32)  4.85 us
    dot_general x1, matrix products, run_expert(): jnp.dot(activated, down_matrix, preferred_element_type=jnp.float32)  4.82 us
    dot_general x1, matrix products, run_expert(): gate_value = jnp.dot(rows, gate_matrix, preferred_element_type=jnp.float32)  4.14 us
  transfers between devices with their start and end apart: 4, of which 2 were waited for; matrix products, arithmetic and copies ran while one was open for 1% of the time, Pallas kernels for 0%

profile of v1, /device:TPU:0, one launch (start us, length us, event | category | flops | bytes accessed | tf_op | source)
XLA Modules:
  0.0 203.7 jit_solution(2837831111134586921)
XLA Ops:
  0.0 0.0 copy-start.2
  0.0 0.0 copy-start.1
  0.0 0.9 slice.31
  0.9 4.9 %collective-permute-start.1 = (s32[16]{0:T(128)S(1)}, s32[16]{0:T(128)S(1)}, u32[]{:S(2)}, u32[]{:S(2)}) collective-permute-start(s32[16]{0:T(128)S(1)} %slice.31), channel_id=1, source_target_pairs={{0,4},{4,8},{8,12},{12,16},{16,20},{20,24},{24,28},{1,5},{5,9},{9,... | collective-permute-start | bytes 200 | tf_op jit(solution)/shard_map/ppermute | solution.py:39
  5.8 0.7 slice.30
  6.5 3.4 %collective-permute-start = (bf16[16,512]{1,0:T(8,128)(2,1)S(1)}, bf16[16,512]{1,0:T(8,128)(2,1)S(1)}, u32[]{:S(2)}, u32[]{:S(2)}) collective-permute-start(bf16[16,512]{1,0:T(8,128)(2,1)S(1)} %slice.30), channel_id=1, source_target_pairs={{0,4},{4,8},{8,12},{12,16},{16,20},{20,24},{24,28},{1,5},{5,9},{9,... | collective-permute-start | bytes 49160 | tf_op jit(solution)/shard_map/ppermute | solution.py:38
  10.0 0.7 convert_reduce_fusion
  10.7 0.1 fusion.37
  10.8 0.0 collective-permute-done.1
  10.8 0.8 pad_add_fusion
  11.6 0.0 collective-permute-done.refs_0_
  11.6 0.0 copy-start.3
  11.6 0.8 broadcast_in_dim.27.refs_2_
  12.4 0.0 copy-done.3
  12.4 3.3 %pool.1 = bf16[512,512]{1,0:T(8,128)(2,1)} custom-call(bf16[16,512]{1,0:T(8,128)(2,1)} %copy-done.3, bf16[512,512]{1,0:T(8,128)(2,1)} %refs_1_.1, s32[528,128]{1,0:T(8,128)} %broadcast_in_dim.27.refs_2_), custom_call_target="tpu_custom_call" | custom-call | tf_op jit(solution)/shard_map/pool/pallas_call | solution.py:43
  15.7 0.0 copy-start.9
  15.7 0.0 copy-start.10
  15.7 2.1 %copy.22 = bf16[4,128,512]{1,2,0:T(8,128)(2,1)} copy(bf16[4,128,512]{2,1,0:T(8,128)(2,1)} %bitcast.50) | data formatting | bytes 1048576 | tf_op jit(solution)/shard_map/all_to_all | solution.py:68
  17.8 3.5 %all-to-all-start = ((bf16[4,128,512]{1,2,0:T(8,128)(2,1)}), bf16[4,128,512]{1,2,0:T(8,128)(2,1)S(1)}, u32[]{:S(2)}, u32[]{:S(2)}) async-start(bf16[4,128,512]{1,2,0:T(8,128)(2,1)} %copy.22), calls=%async_computation | async-start | bytes 1048576 | tf_op jit(solution)/shard_map/all_to_all | solution.py:68
  21.2 0.0 copy-done.2
  21.3 0.3 fusion.14
  21.6 8.5 %all-to-all-done = bf16[4,128,512]{1,2,0:T(8,128)(2,1)S(1)} async-done(((bf16[4,128,512]{1,2,0:T(8,128)(2,1)}), bf16[4,128,512]{1,2,0:T(8,128)(2,1)S(1)}, u32[]{:S(2)}, u32[]{:S(2)}) %all-to-all-start) | async-done | bytes 524320 | tf_op jit(solution)/shard_map/all_to_all | solution.py:68
  30.0 0.0 copy-done.1
  30.0 0.2 fusion.17
  30.3 0.3 fusion.19
  30.5 0.3 fusion.21
  30.8 0.3 fusion.23
  31.0 0.0 copy-done.9
  31.0 0.0 copy-done.10
  31.1 0.0 copy-start.4
  31.1 4.9 %multiply_reduce_fusion = (f32[128]{0:T(128)S(1)}, f32[128,2048]{1,0:T(8,128)S(1)}) fusion(bf16[2048,2048]{1,0:T(8,128)(2,1)} %param.17, f32[128,512]{1,0:T(8,128)S(1)} %fusion.17, f32[128,512]{1,0:T(8,128)S(1)} %fusion.19, f32[128,512]{1,0:T(8,128)S(1)} %fusion.21, f32[128,512]{1,0:T(8,128)S(1)} %fusion.23, f32[2048]{0:T(1024)S(1)} %copy-done.10, ...), kind=kOutput, calls=%fused_computation.20 | convolution fusion | flops 1076625280 | bytes 11018752 | tf_op jit(solution)/shard_map/dot_general | solution.py:82
  35.9 0.0 copy-done.4
  36.0 1.1 convolution_convert_fusion
  37.0 0.0 copy-start.6
  37.0 76.4 %all_to_all.29 = bf16[32,24,2048]{2,1,0:T(8,128)(2,1)S(1)} all-to-all(bf16[32,24,2048]{2,1,0:T(8,128)(2,1)S(1)} %bitcast.42), channel_id=1, replica_groups=mesh['sp'=8,'tp'=4] {'sp','tp'}, dimensions={0} | all-to-all | bytes 6291456 | tf_op jit(solution)/shard_map/all_to_all | solution.py:128
  113.4 0.0 copy-done
  113.4 0.0 copy-done.6
  113.4 3.4 %fusion.2 = f32[768,1024]{1,0:T(8,128)S(1)} fusion(bf16[768,2048]{1,0:T(8,128)(2,1)S(1)} %bitcast.44, bf16[1,2048,1024]{2,1,0:T(8,128)(2,1)S(1)} %copy-done.6), kind=kOutput, calls=%fused_computation.2 | convolution fusion | flops 3221225472 | bytes 10485760 | tf_op jit(solution)/shard_map/dot_general | solution.py:89
  116.8 0.0 copy-done.7
  116.8 0.0 copy-start.8
  116.8 4.1 %multiply_convert_fusion = bf16[768,1024]{1,0:T(8,128)(2,1)S(1)} fusion(f32[768,1024]{1,0:T(8,128)S(1)} %fusion.2, bf16[768,2048]{1,0:T(8,128)(2,1)S(1)} %bitcast.45, bf16[1,2048,1024]{2,1,0:T(8,128)(2,1)S(1)} %copy-done.7), kind=kOutput, calls=%fused_computation.8 | convolution fusion | flops 3229089792 | bytes 12058624 | tf_op jit(solution)/shard_map/dot_general | solution.py:88
  121.0 0.0 copy-done.8
  121.0 4.8 %fusion.6 = bf16[768,2048]{1,0:T(8,128)(2,1)} fusion(bf16[768,1024]{1,0:T(8,128)(2,1)S(1)} %multiply_convert_fusion, bf16[1,1024,2048]{2,1,0:T(8,128)(2,1)S(1)} %copy-done.8), kind=kOutput, calls=%fused_computation.6 | convolution fusion | flops 3222798336 | bytes 8912896 | tf_op jit(solution)/shard_map/dot_general | solution.py:95
  125.8 3.7 %all-to-all-start.2 = ((bf16[32,24,2048]{2,1,0:T(8,128)(2,1)}), bf16[32,24,2048]{2,1,0:T(8,128)(2,1)S(1)}, u32[]{:S(2)}, u32[]{:S(2)}) async-start(bf16[32,24,2048]{2,1,0:T(8,128)(2,1)} %bitcast.43), calls=%async_computation.2 | async-start | bytes 6291456 | tf_op jit(solution)/shard_map/all_to_all | solution.py:128
  129.5 0.0 copy-done.5
  129.5 0.2 select_reduce_fusion
  129.7 71.4 %all-to-all-done.2 = bf16[32,24,2048]{2,1,0:T(8,128)(2,1)S(1)} async-done(((bf16[32,24,2048]{2,1,0:T(8,128)(2,1)}), bf16[32,24,2048]{2,1,0:T(8,128)(2,1)S(1)}, u32[]{:S(2)}, u32[]{:S(2)}) %all-to-all-start.2) | async-done | bytes 3145760 | tf_op jit(solution)/shard_map/all_to_all | solution.py:128
  201.1 2.6 %fusion.11 = bf16[128,2048]{1,0:T(8,128)(2,1)} fusion(f32[128,2048]{1,0:T(8,128)} %copy-done, bf16[768,2048]{1,0:T(8,128)(2,1)S(1)} %bitcast.41, bf16[128,768]{1,0:T(8,128)(2,1)S(1)} %select_reduce_fusion), kind=kOutput, calls=%fused_computation.13 | convolution fusion | flops 403177472 | bytes 4915200 | tf_op jit(solution)/shard_map/dot_general | solution.py:137
  (7 shorter events, 0.0 us)
Async XLA Ops:
  0.0 21.2 %copy-start.2 = (s32[128,4]{0,1:T(4,128)S(1)}, s32[128,4]{0,1:T(4,128)}, u32[]{:S(2)}) copy-start(s32[128,4]{0,1:T(4,128)} %param.19) | copy-start | bytes 6148
  0.0 30.0 %copy-start.1 = (bf16[4,512,512]{2,1,0:T(8,128)(2,1)S(1)}, bf16[4,512,512]{2,1,0:T(8,128)(2,1)}, u32[]{:S(2)}) copy-start(bf16[4,512,512]{2,1,0:T(8,128)(2,1)} %param.15) | copy-start | bytes 6291460
  0.9 9.9 %collective-permute-start.1 = (s32[16]{0:T(128)S(1)}, s32[16]{0:T(128)S(1)}, u32[]{:S(2)}, u32[]{:S(2)}) collective-permute-start(s32[16]{0:T(128)S(1)} %slice.31), channel_id=1, source_target_pairs={{0,4},{4,8},{8,12},{12,16},{16,20},{20,24},{24,28},{1,5},{5,9},{9,... | collective-permute-start | bytes 200 | tf_op jit(solution)/shard_map/ppermute | solution.py:39
  6.5 5.1 %collective-permute-start = (bf16[16,512]{1,0:T(8,128)(2,1)S(1)}, bf16[16,512]{1,0:T(8,128)(2,1)S(1)}, u32[]{:S(2)}, u32[]{:S(2)}) collective-permute-start(bf16[16,512]{1,0:T(8,128)(2,1)S(1)} %slice.30), channel_id=1, source_target_pairs={{0,4},{4,8},{8,12},{12,16},{16,20},{20,24},{24,28},{1,5},{5,9},{9,... | collective-permute-start | bytes 49160 | tf_op jit(solution)/shard_map/ppermute | solution.py:38
  11.6 0.8 copy-start.3
  15.7 15.4 %copy-start.9 = (bf16[128,2048]{1,0:T(8,128)(2,1)S(1)}, bf16[128,2048]{1,0:T(8,128)(2,1)}, u32[]{:S(2)}) copy-start(bf16[128,2048]{1,0:T(8,128)(2,1)} %param.12) | copy-start | bytes 1572868
  15.7 15.4 %copy-start.10 = (f32[2048]{0:T(1024)S(1)}, f32[2048]{0:T(1024)}, u32[]{:S(2)}) copy-start(f32[2048]{0:T(1024)} %param.16) | copy-start | bytes 24580
  17.8 12.3 %all-to-all-start = ((bf16[4,128,512]{1,2,0:T(8,128)(2,1)}), bf16[4,128,512]{1,2,0:T(8,128)(2,1)S(1)}, u32[]{:S(2)}, u32[]{:S(2)}) async-start(bf16[4,128,512]{1,2,0:T(8,128)(2,1)} %copy.22), calls=%async_computation | async-start | bytes 1048576 | tf_op jit(solution)/shard_map/all_to_all | solution.py:68
  31.1 4.9 %copy-start.4 = (f32[2048]{0:T(1024)S(1)}, f32[2048]{0:T(1024)}, u32[]{:S(2)}) copy-start(f32[2048]{0:T(1024)} %param.18) | copy-start | bytes 24580
  35.9 77.5 %copy-start = (f32[128,2048]{1,0:T(8,128)}, f32[128,2048]{1,0:T(8,128)S(1)}, u32[]{:S(2)}) copy-start(f32[128,2048]{1,0:T(8,128)S(1)} %get-tuple-element.6) | copy-start | bytes 3145732
  37.0 76.4 %copy-start.6 = (bf16[1,2048,1024]{2,1,0:T(8,128)(2,1)S(1)}, bf16[1,2048,1024]{2,1,0:T(8,128)(2,1)}, u32[]{:S(2)}) copy-start(bf16[1,2048,1024]{2,1,0:T(8,128)(2,1)} %param.22) | copy-start | bytes 12582916
  113.4 3.4 %copy-start.7 = (bf16[1,2048,1024]{2,1,0:T(8,128)(2,1)S(1)}, bf16[1,2048,1024]{2,1,0:T(8,128)(2,1)}, u32[]{:S(2)}) copy-start(bf16[1,2048,1024]{2,1,0:T(8,128)(2,1)} %param.21) | copy-start | bytes 12582916
  116.8 4.2 %copy-start.8 = (bf16[1,1024,2048]{2,1,0:T(8,128)(2,1)S(1)}, bf16[1,1024,2048]{2,1,0:T(8,128)(2,1)}, u32[]{:S(2)}) copy-start(bf16[1,1024,2048]{2,1,0:T(8,128)(2,1)} %param.23) | copy-start | bytes 12582916
  125.8 3.7 %copy-start.5 = (f32[128,4]{0,1:T(4,128)S(1)}, f32[128,4]{0,1:T(4,128)}, u32[]{:S(2)}) copy-start(f32[128,4]{0,1:T(4,128)} %param.20) | copy-start | bytes 6148
  125.8 75.3 %all-to-all-start.2 = ((bf16[32,24,2048]{2,1,0:T(8,128)(2,1)}), bf16[32,24,2048]{2,1,0:T(8,128)(2,1)S(1)}, u32[]{:S(2)}, u32[]{:S(2)}) async-start(bf16[32,24,2048]{2,1,0:T(8,128)(2,1)} %bitcast.43), calls=%async_computation.2 | async-start | bytes 6291456 | tf_op jit(solution)/shard_map/all_to_all | solution.py:128

commit v2 on v1

--- a/solution.py
+++ b/solution.py
@@ -84,15 +84,414 @@
     return resid, rms_scale(resid, ffn_gain)
 
 
-def run_expert(rows, gate_matrix, up_matrix, down_matrix):
-    gate_value = jnp.dot(rows, gate_matrix, preferred_element_type=jnp.float32)
-    up_value = jnp.dot(rows, up_matrix, preferred_element_type=jnp.float32)
-    gated = jnp.minimum(gate_value, clamp_limit)
-    linear = jnp.clip(up_value, -clamp_limit, clamp_limit)
-    activated = (gated * jax.nn.sigmoid(sigmoid_alpha * gated) * (linear + 1.0)).astype(
-        jnp.bfloat16
+CHUNKS = 4
+
+
+def experts_kernel(
+    z_count,
+    x_count,
+    tp_count,
+    normed_ref,
+    resid_ref,
+    select_ref,
+    weigh_ref,
+    gate_hbm,
+    up_hbm,
+    down_hbm,
+    out_ref,
+    gate_ref,
+    up_ref,
+    down_ref,
+    column,
+    outgoing,
+    rows,
+    gate_sum,
+    up_sum,
+    activated,
+    results,
+    returned,
+    part,
+    right_out,
+    left_out,
+    right_in,
+    left_in,
+    load_sem,
+    col_send,
+    col_recv,
+    plane_send,
+    plane_recv,
+    back_send,
+    back_recv,
+    sum_send,
+    sum_recv,
+):
+    sp, tp = lax.axis_index("sp"), lax.axis_index("tp")
+    z, x = lax.div(sp, x_count), lax.rem(sp, x_count)
+    plane = x_count * tp_count
+    place = x * tp_count + tp
+    tok, width = normed_ref.shape
+    wide = width // CHUNKS
+    share = select_ref.shape[0] // plane
+    tile = min(256, wide)
+    last = z_count - 1
+    has_right, has_left = z < last, z > 0
+
+    def at_z(step):
+        return {"sp": sp + step * x_count, "tp": tp}
+
+    def at_plane(other):
+        return {"sp": z * x_count + lax.div(other, tp_count), "tp": lax.rem(other, tp_count)}
+
+    def remote(src, dst, send, recv, device):
+        return pltpu.make_async_remote_copy(
+            src_ref=src,
+            dst_ref=dst,
+            send_sem=send,
+            recv_sem=recv,
+            device_id=device,
+            device_id_type=pl.DeviceIdType.MESH,
+        )
+
+    def cols_of(k):
+        return pl.ds(pl.multiple_of(k * wide, wide), wide)
+
+    def share_of(i):
+        return pl.ds(pl.multiple_of(i * share, share), share)
+
+    loads = [
+        pltpu.make_async_copy(src, dst, load_sem.at[i])
+        for i, (src, dst) in enumerate(
+            ((gate_hbm, gate_ref), (up_hbm, up_ref), (down_hbm, down_ref))
+        )
+    ]
+
+    barrier = pltpu.get_barrier_semaphore()
+
+    def greet(device):
+        pl.semaphore_signal(barrier, inc=1, device_id=device, device_id_type=pl.DeviceIdType.MESH)
+
+    pl.when(has_right)(lambda: greet(at_z(1)))
+    pl.when(has_left)(lambda: greet(at_z(-1)))
+
+    @pl.loop(1, plane)
+    def _(i):
+        greet(at_plane(lax.rem(place + i, plane)))
+
+    for load in loads:
+        load.start()
+    gate_sum[...] = jnp.zeros_like(gate_sum)
+    up_sum[...] = jnp.zeros_like(up_sum)
+    pl.semaphore_wait(
+        barrier, plane - 1 + has_right.astype(jnp.int32) + has_left.astype(jnp.int32)
     )
-    return jnp.dot(activated, down_matrix, preferred_element_type=jnp.float32).astype(jnp.bfloat16)
+
+    def to_right(k, e):
+        src = normed_ref.at[:, cols_of(k)] if e == 0 else column.at[k, e - 1]
+        return remote(
+            src, column.at[k, e], col_send.at[k, 0, e], col_recv.at[k, e], at_z(1)
+        )
+
+    def to_left(k, e):
+        src = normed_ref.at[:, cols_of(k)] if e == 0 else column.at[k, z_count - e - 1]
+        back = z_count - e - 2
+        return remote(
+            src, column.at[k, back], col_send.at[k, 1, e], col_recv.at[k, back], at_z(-1)
+        )
+
+    def send_own(k):
+        pl.when(has_right)(lambda: to_right(k, 0).start())
+        pl.when(has_left)(lambda: to_left(k, 0).start())
+
+    def relay(k):
+        for e in range(1, z_count):
+
+            @pl.when(z >= e)
+            def _():
+                to_right(k, e - 1).wait_recv()
+                if e < last:
+                    pl.when(has_right)(lambda: to_right(k, e).start())
+
+            @pl.when(last - z >= e)
+            def _():
+                to_left(k, e - 1).wait_recv()
+                if e < last:
+                    pl.when(has_left)(lambda: to_left(k, e).start())
+
+    def to_expert(k, i):
+        other = lax.rem(place + i, plane)
+        return remote(
+            outgoing.at[k, share_of(other)],
+            rows.at[k, share_of(i)],
+            plane_send.at[k, i - 1],
+            plane_recv.at[k, i - 1],
+            at_plane(other),
+        )
+
+    def dispatch(k):
+        own = jnp.dot(
+            select_ref[:, :tok], normed_ref[:, cols_of(k)], preferred_element_type=jnp.float32
+        )
+        others = jnp.dot(
+            select_ref[:, tok:],
+            column[k].reshape(last * tok, wide),
+            preferred_element_type=jnp.float32,
+        )
+        outgoing[k] = (own + others).astype(jnp.bfloat16)
+
+        @pl.loop(1, plane)
+        def _(i):
+            to_expert(k, i).start()
+
+        rows[k, pl.ds(0, share)] = outgoing[k, share_of(place)]
+
+    def accumulate(k):
+        @pl.loop(1, plane)
+        def _(i):
+            to_expert(k, i).wait_recv()
+
+        @pl.loop(0, gate_ref.shape[1] // tile)
+        def _(n):
+            cols = pl.ds(pl.multiple_of(n * tile, tile), tile)
+            gate_sum[:, cols] += jnp.dot(
+                rows[k], gate_ref[cols_of(k), cols], preferred_element_type=jnp.float32
+            )
+            up_sum[:, cols] += jnp.dot(
+                rows[k], up_ref[cols_of(k), cols], preferred_element_type=jnp.float32
+            )
+
+    send_own(0)
+
+    @pl.loop(0, CHUNKS)
+    def _(k):
+        pl.when(k + 1 < CHUNKS)(lambda: send_own(k + 1))
+        relay(k)
+        dispatch(k)
+
+        @pl.when(k == 1)
+        def _():
+            loads[0].wait()
+            loads[1].wait()
+
+        pl.when(k > 0)(lambda: accumulate(k - 1))
+
+    accumulate(CHUNKS - 1)
+
+    @pl.loop(0, gate_ref.shape[1] // tile)
+    def _(n):
+        cols = pl.ds(pl.multiple_of(n * tile, tile), tile)
+        gated = jnp.minimum(gate_sum[:, cols], clamp_limit)
+        linear = jnp.clip(up_sum[:, cols], -clamp_limit, clamp_limit)
+        activated[:, cols] = (
+            gated * jax.nn.sigmoid(sigmoid_alpha * gated) * (linear + 1.0)
+        ).astype(jnp.bfloat16)
+
+    loads[2].wait()
+
+    def to_relay(k, i):
+        return remote(
+            results.at[k, share_of(i)],
+            returned.at[k, share_of(place)],
+            back_send.at[k, i - 1],
+            back_recv.at[k, i - 1],
+            at_plane(lax.rem(place + plane - i, plane)),
+        )
+
+    @pl.loop(0, CHUNKS)
+    def _(k):
+        @pl.loop(0, wide // tile)
+        def _(n):
+            cols = pl.ds(pl.multiple_of(n * tile, tile), tile)
+            from_cols = pl.ds(pl.multiple_of(k * wide + n * tile, tile), tile)
+            results[k, :, cols] = jnp.dot(
+                activated[...], down_ref[:, from_cols], preferred_element_type=jnp.float32
+            ).astype(jnp.bfloat16)
+
+        @pl.loop(1, plane)
+        def _(i):
+            to_relay(k, i).start()
+
+        returned[k, share_of(place)] = results[k, pl.ds(0, share)]
+
+    def combine(k):
+        @pl.loop(1, plane)
+        def _(i):
+            to_relay(k, i).wait_recv()
+
+        part[k] = jnp.dot(weigh_ref[...], returned[k], preferred_element_type=jnp.float32)
+
+    def sum_right(k, e):
+        return remote(
+            right_out.at[k, e - 1],
+            right_in.at[k, e - 1],
+            sum_send.at[k, 0, e - 1],
+            sum_recv.at[k, 0, e - 1],
+            at_z(1),
+        )
+
+    def sum_left(k, e):
+        return remote(
+            left_out.at[k, e - 1],
+            left_in.at[k, e - 1],
+            sum_send.at[k, 1, e - 1],
+            sum_recv.at[k, 1, e - 1],
+            at_z(-1),
+        )
+
+    def add_up(k):
+        for e in range(last, 0, -1):
+
+            @pl.when(z + e <= last)
+            def _():
+                mine = slice((z_count - e) * tok, (z_count - e + 1) * tok)
+                if e < last:
+
+                    @pl.when(has_left)
+                    def _():
+                        sum_right(k, e + 1).wait_recv()
+                        part[k, mine] += right_in[k, e].astype(jnp.float32)
+
+                right_out[k, e - 1] = part[k, mine].astype(jnp.bfloat16)
+                sum_right(k, e).start()
+
+            @pl.when(z >= e)
+            def _():
+                mine = slice(e * tok, (e + 1) * tok)
+                if e < last:
+
+                    @pl.when(has_right)
+                    def _():
+                        sum_left(k, e + 1).wait_recv()
+                        part[k, mine] += left_in[k, e].astype(jnp.float32)
+
+                left_out[k, e - 1] = part[k, mine].astype(jnp.bfloat16)
+                sum_left(k, e).start()
+
+    def finish(k):
+        own = slice(0, tok)
+
+        @pl.when(has_left)
+        def _():
+            sum_right(k, 1).wait_recv()
+            part[k, own] += right_in[k, 0].astype(jnp.float32)
+
+        @pl.when(has_right)
+        def _():
+            sum_left(k, 1).wait_recv()
+            part[k, own] += left_in[k, 0].astype(jnp.float32)
+
+        out_ref[:, cols_of(k)] = (
+            resid_ref[:, cols_of(k)].astype(jnp.float32) + part[k, own]
+        ).astype(jnp.bfloat16)
+
+    combine(0)
+
+    @pl.loop(0, CHUNKS)
+    def _(k):
+        pl.when(k + 1 < CHUNKS)(lambda: combine(k + 1))
+        add_up(k)
+        pl.when(k > 0)(lambda: finish(k - 1))
+
+    finish(CHUNKS - 1)
+
+    @pl.loop(0, CHUNKS)
+    def _(k):
+        for e in range(last):
+
+            @pl.when((z >= e) & has_right)
+            def _():
+                to_right(k, e).wait_send()
+
+            @pl.when((last - z >= e) & has_left)
+            def _():
+                to_left(k, e).wait_send()
+
+        for e in range(1, z_count):
+            pl.when(z + e <= last)(lambda: sum_right(k, e).wait_send())
+            pl.when(z >= e)(lambda: sum_left(k, e).wait_send())
+
+        @pl.loop(1, plane)
+        def _(i):
+            to_expert(k, i).wait_send()
+            to_relay(k, i).wait_send()
+
+
+def run_experts(normed, resid, routes, route_weights, gate, up, down):
+    tok, width = normed.shape
+    sp_count, tp_count = lax.axis_size("sp"), lax.axis_size("tp")
+    x_count = max(tp_count // 2, 1)
+    z_count = sp_count // x_count
+    plane = x_count * tp_count
+    top_count = routes.shape[1]
+    hidden = gate.shape[1]
+    capacity = 3 * tok * top_count // (2 * plane * z_count)
+    share = -(-z_count * capacity // 16) * 16
+    slots = slots_of(routes, plane * z_count, capacity)
+    info = jnp.concatenate([slots.astype(jnp.float32), route_weights], 1)
+    z = lax.axis_index("sp") // x_count
+    slot_ids = jnp.arange(plane * share, dtype=jnp.int32)
+    targets, weights = [], []
+    for d in range(z_count):
+        here = info
+        if d:
+            onward = [(s, (s + d * x_count) % sp_count) for s in range(sp_count)]
+            here = lax.ppermute(info, "sp", onward)
+        local = here[:, :top_count].astype(jnp.int32) - z * plane * capacity
+        inside = (local >= 0) & (local < plane * capacity)
+        target = local // capacity * share + d * capacity + local % capacity
+        targets.append(jnp.where(inside, target, -1))
+        weights.append(here[:, top_count:])
+    target, weight = jnp.concatenate(targets), jnp.concatenate(weights)
+    target_t = target.T
+    select, weigh = False, 0.0
+    for j in range(top_count):
+        select = select | (slot_ids[:, None] == target_t[j][None, :])
+        weigh = weigh + jnp.where(target[:, j, None] == slot_ids[None, :], weight[:, j, None], 0.0)
+    select, weigh = select.astype(jnp.bfloat16), weigh.astype(jnp.bfloat16)
+    wide = width // CHUNKS
+    last = z_count - 1
+    bf, f32 = jnp.bfloat16, jnp.float32
+    vmem = pl.BlockSpec(memory_space=pltpu.VMEM)
+    hbm = pl.BlockSpec(memory_space=pl.ANY)
+    dma = pltpu.SemaphoreType.DMA
+    slab = pltpu.VMEM((CHUNKS, plane * share, wide), bf)
+    hop = pltpu.VMEM((CHUNKS, last, tok, wide), bf)
+    return pl.pallas_call(
+        lambda *refs: experts_kernel(z_count, x_count, tp_count, *refs),
+        out_shape=jax.ShapeDtypeStruct((tok, width), bf),
+        in_specs=[vmem] * 4 + [hbm] * 3,
+        out_specs=vmem,
+        scratch_shapes=[
+            pltpu.VMEM((width, hidden), bf),
+            pltpu.VMEM((width, hidden), bf),
+            pltpu.VMEM((hidden, width), bf),
+            hop,
+            slab,
+            slab,
+            pltpu.VMEM((plane * share, hidden), f32),
+            pltpu.VMEM((plane * share, hidden), f32),
+            pltpu.VMEM((plane * share, hidden), bf),
+            slab,
+            slab,
+            pltpu.VMEM((CHUNKS, z_count * tok, wide), f32),
+            hop,
+            hop,
+            hop,
+            hop,
+            dma((3,)),
+            dma((CHUNKS, 2, last)),
+            dma((CHUNKS, last)),
+            dma((CHUNKS, plane - 1)),
+            dma((CHUNKS, plane - 1)),
+            dma((CHUNKS, plane - 1)),
+            dma((CHUNKS, plane - 1)),
+            dma((CHUNKS, 2, last)),
+            dma((CHUNKS, 2, last)),
+        ],
+        compiler_params=pltpu.CompilerParams(
+            collective_id=0, has_side_effects=True, vmem_limit_bytes=65000 * 1024
+        ),
+        name="experts",
+    )(normed, resid, select, weigh, gate, up, down)
 
 
 def body(
@@ -109,33 +508,11 @@
     expert_up,
     expert_down,
 ):
-    tok_count, model_width = stream.shape
-    expert_count = lax.axis_size("sp") * lax.axis_size("tp")
-    top_count = routes.shape[1]
-    capacity = 3 * tok_count * top_count // (2 * expert_count)
     mixed = pool(projected, segments, group_weight.shape[1])
-    slots = slots_of(routes, expert_count, capacity)
     resid, normed = mixer(mixed, stream, group_weight, group_scale, out_weight, ffn_gain)
-    slot_ids = jnp.arange(expert_count * capacity, dtype=jnp.int32)
-    chosen = slots[:, :, None] == slot_ids
-    select = jnp.any(chosen, 1).astype(jnp.bfloat16)
-    weigh = jnp.sum(jnp.where(chosen, route_weights[:, :, None], 0.0), 1).astype(jnp.bfloat16)
-    outgoing = lax.dot_general(
-        select, normed, (((0,), (0,)), ((), ())), preferred_element_type=jnp.float32
-    ).astype(jnp.bfloat16)
-
-    def exchange(rows):
-        return lax.all_to_all(
-            rows.reshape(expert_count, capacity, model_width),
-            ("sp", "tp"),
-            split_axis=0,
-            concat_axis=0,
-            tiled=True,
-        ).reshape(expert_count * capacity, model_width)
-
-    results = run_expert(exchange(outgoing), expert_gate[0], expert_up[0], expert_down[0])
-    moe_sum = jnp.dot(weigh, exchange(results), preferred_element_type=jnp.float32)
-    return (resid.astype(jnp.float32) + moe_sum).astype(jnp.bfloat16)
+    return run_experts(
+        normed, resid, routes, route_weights, expert_gate[0], expert_up[0], expert_down[0]
+    )
 
 
 def solution(mesh):

time: 204 us -> 174 us (0.85)
  Pallas kernels: 3.25 us -> 127 us
  blocking collectives: 76.4 us -> 0 us
  waiting for transfers between devices: 79.8 us -> 7.08 us
  matrix products: 22 us -> 5.99 us
  other arithmetic: 2 us -> 8.53 us
  local copies, waits for them, and re-layouts: 4.59 us -> 7.5 us
    pallas_call x0 -> x1, Pallas kernels: none -> 123 us  [run_experts(): pl.pallas_call(lambda *refs: experts_kernel(z_count, x_count, tp_count, *...]
    all_to_all x1 -> x0, blocking collectives: 76.4 us -> none  [exchange(): lax.all_to_all(rows.reshape(expert_count, capacity, model_width), ('sp',...]
    all_to_all x1 -> x0, waiting for transfers between devices: 71.4 us -> none  [exchange(): lax.all_to_all(rows.reshape(expert_count, capacity, model_width), ('sp',...]
    dot_general x5 -> x0, matrix products: 16 us -> none  [the longest x1 4.82 us: run_expert(): jnp.dot(activated, down_matrix, preferred_element_type=jnp.float32)]
    ppermute x0 -> x3, starting transfers between devices: none -> 6.09 us  [run_experts(): here = lax.ppermute(info, 'sp', onward)]
    convert_element_type x0 -> x3, other arithmetic: none -> 4.19 us  [the longest x2 3.21 us: run_experts(): select, weigh = (select.astype(jnp.bfloat16), weigh.astype(jnp.bfloat16))]
    all_to_all x1 -> x0, starting transfers between devices: 3.66 us -> none  [exchange(): lax.all_to_all(rows.reshape(expert_count, capacity, model_width), ('sp',...]
    unnamed x22 -> x13, local copies, waits for them, and re-layouts: 0.05 us -> 2.95 us
  transfers between devices with their start and end apart: 4 -> 6, of which waited for: 2 -> 1; matrix products, arithmetic and copies ran while one was open for 1% -> 4% of each run, Pallas kernels for 0% -> 0%
where the time goes in v2:
time: 174 us; the launch traced here: 173 us
  Pallas kernels  127 us (73%)
  starting transfers between devices  17.3 us (10%)
  other arithmetic  8.53 us (5%)
  local copies, waits for them, and re-layouts  7.5 us (4%)
  waiting for transfers between devices  7.08 us (4%)
  matrix products  5.99 us (3%)
    pallas_call x1, Pallas kernels, run_experts(): pl.pallas_call(lambda *refs: experts_kernel(z_count, x_count, tp_count, *...  123 us
    all_to_all x1, waiting for transfers between devices, mixer(): lax.all_to_all(mixed, 'tp', split_axis=0, concat_axis=1, tiled=True)  7.06 us
    ppermute x3, starting transfers between devices, run_experts(): here = lax.ppermute(info, 'sp', onward)  6.09 us
    dot_general x1, matrix products, mixer(): mixer_out = jnp.dot(scaled, out_weight, preferred_element_type=jnp.float32)  4.85 us
    ppermute x1, starting transfers between devices, pool(): halo = lax.ppermute(projected[row_count - longest_window:], 'sp', onward)  4.34 us
  transfers between devices with their start and end apart: 6, of which 1 were waited for; matrix products, arithmetic and copies ran while one was open for 4% of the time, Pallas kernels for 0%

profile of v2, /device:TPU:0, one launch (start us, length us, event | category | flops | bytes accessed | tf_op | source)
XLA Modules:
  0.0 173.1 jit_solution(7747552964149716530)
XLA Ops:
  0.0 0.7 convert_reduce_fusion
  0.7 0.1 fusion.27
  0.8 0.7 select_reduce_fusion
  1.6 0.7 fusion.30
  2.3 0.7 pad_maximum_fusion.1
  3.0 5.1 %collective-permute-start.4 = (f32[128,8]{0,1:T(8,128)S(1)}, f32[128,8]{0,1:T(8,128)S(1)}, u32[]{:S(2)}, u32[]{:S(2)}) collective-permute-start(f32[128,8]{0,1:T(8,128)S(1)} %pad_maximum_fusion.1), channel_id=1, source_target_pairs={{0,24},{4,28},{8,0},{12,4},{16,8},{20,12},{24,16},{28,20},{1,25},{... | collective-permute-start | bytes 12296 | tf_op jit(solution)/shard_map/ppermute | solution.py:437
  8.0 0.0 collective-permute-start.3
  8.1 1.0 collective-permute-start.2
  9.1 0.8 slice.85
  9.8 3.4 %collective-permute-start.1 = (s32[16]{0:T(128)S(1)}, s32[16]{0:T(128)S(1)}, u32[]{:S(2)}, u32[]{:S(2)}) collective-permute-start(s32[16]{0:T(128)S(1)} %slice.85), channel_id=1, source_target_pairs={{0,4},{4,8},{8,12},{12,16},{16,20},{20,24},{24,28},{1,5},{5,9},{9,... | collective-permute-start | bytes 200 | tf_op jit(solution)/shard_map/ppermute | solution.py:39
  13.2 0.7 slice.84
  13.9 4.3 %collective-permute-start = (bf16[16,512]{1,0:T(8,128)(2,1)S(1)}, bf16[16,512]{1,0:T(8,128)(2,1)S(1)}, u32[]{:S(2)}, u32[]{:S(2)}) collective-permute-start(bf16[16,512]{1,0:T(8,128)(2,1)S(1)} %slice.84), channel_id=1, source_target_pairs={{0,4},{4,8},{8,12},{12,16},{16,20},{20,24},{24,28},{1,5},{5,9},{9,... | collective-permute-start | bytes 49160 | tf_op jit(solution)/shard_map/ppermute | solution.py:38
  18.3 0.0 collective-permute-done.1
  18.3 0.8 pad_add_fusion.1
  19.1 0.0 collective-permute-done.4
  19.1 0.0 collective-permute-done.3
  19.1 0.0 collective-permute-done.2
  19.2 0.7 pad_maximum_fusion
  19.9 1.5 fusion.4.refs_2_
  21.4 0.0 collective-permute-done.refs_0_
  21.4 0.0 copy-start.2
  21.4 0.8 broadcast_in_dim.82.refs_2_
  22.3 0.0 copy-done.2
  22.3 3.3 %pool.1 = bf16[512,512]{1,0:T(8,128)(2,1)} custom-call(bf16[16,512]{1,0:T(8,128)(2,1)} %copy-done.2, bf16[512,512]{1,0:T(8,128)(2,1)} %refs_1_.1, s32[528,128]{1,0:T(8,128)} %broadcast_in_dim.82.refs_2_), custom_call_target="tpu_custom_call" | custom-call | tf_op jit(solution)/shard_map/pool/pallas_call | solution.py:43
  25.5 0.0 copy-start
  25.5 2.2 %copy.18 = bf16[4,128,512]{1,2,0:T(8,128)(2,1)} copy(bf16[4,128,512]{2,1,0:T(8,128)(2,1)} %bitcast.42) | data formatting | bytes 1048576 | tf_op jit(solution)/shard_map/all_to_all | solution.py:68
  27.7 3.5 %all-to-all-start = ((bf16[4,128,512]{1,2,0:T(8,128)(2,1)}), bf16[4,128,512]{1,2,0:T(8,128)(2,1)S(1)}, u32[]{:S(2)}, u32[]{:S(2)}) async-start(bf16[4,128,512]{1,2,0:T(8,128)(2,1)} %copy.18), calls=%async_computation | async-start | bytes 1048576 | tf_op jit(solution)/shard_map/all_to_all | solution.py:68
  31.2 1.7 add_convert_fusion.refs_3_
  32.9 7.1 %all-to-all-done = bf16[4,128,512]{1,2,0:T(8,128)(2,1)S(1)} async-done(((bf16[4,128,512]{1,2,0:T(8,128)(2,1)}), bf16[4,128,512]{1,2,0:T(8,128)(2,1)S(1)}, u32[]{:S(2)}, u32[]{:S(2)}) %all-to-all-start) | async-done | bytes 524320 | tf_op jit(solution)/shard_map/all_to_all | solution.py:68
  40.0 0.0 copy-done
  40.0 0.2 fusion.10
  40.2 0.0 copy-start.4
  40.3 0.0 copy-start.5
  40.3 0.2 fusion.12
  40.5 0.3 fusion.14
  40.8 0.3 fusion.16
  41.0 0.3 copy-done.4
  41.3 0.0 copy-done.5
  41.3 0.0 copy-start.3
  41.3 4.9 %fusion.5 = (f32[128]{0:T(128)S(1)}, bf16[128,2048]{1,0:T(8,128)(2,1)S(1)}) fusion(bf16[2048,2048]{1,0:T(8,128)(2,1)} %param.17, f32[128,512]{1,0:T(8,128)S(1)} %fusion.10, f32[128,512]{1,0:T(8,128)S(1)} %fusion.12, f32[128,512]{1,0:T(8,128)S(1)} %fusion.14, f32[128,512]{1,0:T(8,128)S(1)} %fusion.16, f32[2048]{0:T(1024)S(1)} %copy-done.5, ...), kind=kOutput, calls=%fused_computation.17 | convolution fusion | flops 1076625280 | bytes 10494464 | tf_op jit(solution)/shard_map/dot_general | solution.py:82
  46.2 0.0 copy-start.1
  46.2 0.8 copy-done.1
  47.0 0.0 copy-done.3
  47.0 1.0 fusion.7.refs_0_
  47.9 123.3 %experts.1 = bf16[128,2048]{1,0:T(8,128)(2,1)} custom-call(bf16[128,2048]{1,0:T(8,128)(2,1)} %fusion.7.refs_0_, bf16[128,2048]{1,0:T(8,128)(2,1)} %copy-done.1, bf16[768,512]{1,0:T(8,128)(2,1)} %fusion.4.refs_2_, bf16[512,768]{1,0:T(8,128)(2,1)} %add_convert_fusion.refs_3_, bf16[2048,1024]{1,0:T(8,128)(2,1)} %bitcast.35, bf16[2048,1024]{1,0:T(8,128)(2,1)} %bitcast.36, ...), custom_call_target="tpu_custom_call" | custom-call | tf_op jit(solution)/shard_map/experts/pallas_call | solution.py:458
  171.2 1.9 %copy.20 = bf16[128,2048]{1,0:T(8,128)(2,1)} copy(bf16[128,2048]{1,0:T(8,128)(2,1)} %experts.1) | data formatting | bytes 1048576
  (12 shorter events, 0.1 us)
Async XLA Ops:
  3.0 16.1 %collective-permute-start.4 = (f32[128,8]{0,1:T(8,128)S(1)}, f32[128,8]{0,1:T(8,128)S(1)}, u32[]{:S(2)}, u32[]{:S(2)}) collective-permute-start(f32[128,8]{0,1:T(8,128)S(1)} %pad_maximum_fusion.1), channel_id=1, source_target_pairs={{0,24},{4,28},{8,0},{12,4},{16,8},{20,12},{24,16},{28,20},{1,25},{... | collective-permute-start | bytes 12296 | tf_op jit(solution)/shard_map/ppermute | solution.py:437
  8.0 11.0 %collective-permute-start.3 = (f32[128,8]{0,1:T(8,128)S(1)}, f32[128,8]{0,1:T(8,128)S(1)}, u32[]{:S(2)}, u32[]{:S(2)}) collective-permute-start(f32[128,8]{0,1:T(8,128)S(1)} %pad_maximum_fusion.1), channel_id=1, source_target_pairs={{0,16},{4,20},{8,24},{12,28},{16,0},{20,4},{24,8},{28,12},{1,17},{... | collective-permute-start | bytes 12296 | tf_op jit(solution)/shard_map/ppermute | solution.py:437
  8.1 11.1 %collective-permute-start.2 = (f32[128,8]{0,1:T(8,128)S(1)}, f32[128,8]{0,1:T(8,128)S(1)}, u32[]{:S(2)}, u32[]{:S(2)}) collective-permute-start(f32[128,8]{0,1:T(8,128)S(1)} %pad_maximum_fusion.1), channel_id=1, source_target_pairs={{0,8},{4,12},{8,16},{12,20},{16,24},{20,28},{24,0},{28,4},{1,9},{5... | collective-permute-start | bytes 12296 | tf_op jit(solution)/shard_map/ppermute | solution.py:437
  9.8 8.5 %collective-permute-start.1 = (s32[16]{0:T(128)S(1)}, s32[16]{0:T(128)S(1)}, u32[]{:S(2)}, u32[]{:S(2)}) collective-permute-start(s32[16]{0:T(128)S(1)} %slice.85), channel_id=1, source_target_pairs={{0,4},{4,8},{8,12},{12,16},{16,20},{20,24},{24,28},{1,5},{5,9},{9,... | collective-permute-start | bytes 200 | tf_op jit(solution)/shard_map/ppermute | solution.py:39
  13.9 7.5 %collective-permute-start = (bf16[16,512]{1,0:T(8,128)(2,1)S(1)}, bf16[16,512]{1,0:T(8,128)(2,1)S(1)}, u32[]{:S(2)}, u32[]{:S(2)}) collective-permute-start(bf16[16,512]{1,0:T(8,128)(2,1)S(1)} %slice.84), channel_id=1, source_target_pairs={{0,4},{4,8},{8,12},{12,16},{16,20},{20,24},{24,28},{1,5},{5,9},{9,... | collective-permute-start | bytes 49160 | tf_op jit(solution)/shard_map/ppermute | solution.py:38
  21.4 0.9 copy-start.2
  25.5 14.5 %copy-start = (bf16[4,512,512]{2,1,0:T(8,128)(2,1)S(1)}, bf16[4,512,512]{2,1,0:T(8,128)(2,1)}, u32[]{:S(2)}) copy-start(bf16[4,512,512]{2,1,0:T(8,128)(2,1)} %param.15) | copy-start | bytes 6291460
  27.7 12.3 %all-to-all-start = ((bf16[4,128,512]{1,2,0:T(8,128)(2,1)}), bf16[4,128,512]{1,2,0:T(8,128)(2,1)S(1)}, u32[]{:S(2)}, u32[]{:S(2)}) async-start(bf16[4,128,512]{1,2,0:T(8,128)(2,1)} %copy.18), calls=%async_computation | async-start | bytes 1048576 | tf_op jit(solution)/shard_map/all_to_all | solution.py:68
  40.2 1.0 copy-start.4
  40.3 1.0 copy-start.5
  41.3 5.7 %copy-start.3 = (f32[2048]{0:T(1024)S(1)}, f32[2048]{0:T(1024)}, u32[]{:S(2)}) copy-start(f32[2048]{0:T(1024)} %param.18) | copy-start | bytes 24580
  46.2 0.8 copy-start.1

commit v3 on v2

--- a/solution.py
+++ b/solution.py
@@ -31,15 +31,117 @@
         mixed_ref[:, cols] = (total / count - values)[longest_window:].astype(jnp.bfloat16)
 
 
-def pool(projected, segments, group_width):
-    sp_count = lax.axis_size("sp")
+def exchange_kernel(
+    z_count, x_count, sp_count,
+    tail_ref, docs_ref, info_ref, halo_ref, halo_docs_ref, infos_ref,
+    halo, halo_docs, infos, send_sem, recv_sem,
+):
+    sp, tp = lax.axis_index("sp"), lax.axis_index("tp")
+    z, x = lax.div(sp, x_count), lax.rem(sp, x_count)
+    has_next, has_prev = sp < sp_count - 1, sp > 0
+    barrier = pltpu.get_barrier_semaphore()
+
+    def along_z(d):
+        return {"sp": lax.rem(z + d, z_count) * x_count + x, "tp": tp}
+
+    def along_sp(step):
+        return {"sp": sp + step, "tp": tp}
+
+    def greet(device):
+        pl.semaphore_signal(barrier, inc=1, device_id=device, device_id_type=pl.DeviceIdType.MESH)
+
+    def remote(src, dst, i, device):
+        return pltpu.make_async_remote_copy(
+            src_ref=src,
+            dst_ref=dst,
+            send_sem=send_sem.at[i],
+            recv_sem=recv_sem.at[i],
+            device_id=device,
+            device_id_type=pl.DeviceIdType.MESH,
+        )
+
+    pl.when(has_next)(lambda: greet(along_sp(1)))
+    pl.when(has_prev)(lambda: greet(along_sp(-1)))
+    for d in range(1, z_count):
+        greet(along_z(d))
+    pl.semaphore_wait(
+        barrier, z_count - 1 + has_next.astype(jnp.int32) + has_prev.astype(jnp.int32)
+    )
+    tables = [remote(info_ref, infos.at[d - 1], d + 1, along_z(d)) for d in range(1, z_count)]
+    edges = [
+        remote(tail_ref, halo, 0, along_sp(1)),
+        remote(docs_ref, halo_docs, 1, along_sp(1)),
+    ]
+
+    @pl.when(has_next)
+    def _():
+        for copy in edges:
+            copy.start()
+
+    for copy in tables:
+        copy.start()
+    infos_ref[0] = info_ref[...]
+
+    @pl.when(has_prev)
+    def _():
+        for copy in edges:
+            copy.wait_recv()
+        halo_ref[...] = halo[...]
+        halo_docs_ref[...] = halo_docs[...]
+
+    @pl.when(sp == 0)
+    def _():
+        halo_ref[...] = jnp.zeros_like(halo_ref)
+        halo_docs_ref[...] = jnp.full_like(halo_docs_ref, -1)
+
+    for d, copy in enumerate(tables):
+        copy.wait_recv()
+        infos_ref[d + 1] = infos[d]
+
+    @pl.when(has_next)
+    def _():
+        for copy in edges:
+            copy.wait_send()
+
+    for copy in tables:
+        copy.wait_send()
+
+
+def exchange(projected, segments, routes, route_weights):
     row_count, channels = projected.shape
-    onward = [(i, i + 1) for i in range(sp_count - 1)]
-    halo = lax.ppermute(projected[row_count - longest_window :], "sp", onward)
-    halo_docs = lax.ppermute(segments[row_count - longest_window :], "sp", onward)
-    halo_docs = jnp.where(lax.axis_index("sp") == 0, -1, halo_docs)
-    docs = jnp.concatenate([halo_docs, segments])
-    docs = jnp.broadcast_to(docs[:, None], (row_count + longest_window, 128))
+    sp_count, tp_count = lax.axis_size("sp"), lax.axis_size("tp")
+    x_count = max(tp_count // 2, 1)
+    z_count = sp_count // x_count
+    tok, top_count = routes.shape
+    capacity = 3 * tok * top_count // (2 * sp_count * tp_count)
+    slots = slots_of(routes, sp_count * tp_count, capacity)
+    info = jnp.concatenate([slots.astype(jnp.float32), route_weights], 1).T
+    docs = jnp.broadcast_to(segments[:, None], (row_count, 128))
+    edge = (longest_window, channels)
+    halo, halo_docs, infos = pl.pallas_call(
+        lambda *refs: exchange_kernel(z_count, x_count, sp_count, *refs),
+        out_shape=(
+            jax.ShapeDtypeStruct(edge, jnp.bfloat16),
+            jax.ShapeDtypeStruct((longest_window, 128), jnp.int32),
+            jax.ShapeDtypeStruct((z_count, 2 * top_count, tok), jnp.float32),
+        ),
+        in_specs=[pl.BlockSpec(memory_space=pltpu.VMEM)] * 3,
+        out_specs=(pl.BlockSpec(memory_space=pltpu.VMEM),) * 3,
+        scratch_shapes=[
+            pltpu.VMEM(edge, jnp.bfloat16),
+            pltpu.VMEM((longest_window, 128), jnp.int32),
+            pltpu.VMEM((z_count - 1, 2 * top_count, tok), jnp.float32),
+            pltpu.SemaphoreType.DMA((z_count + 1,)),
+            pltpu.SemaphoreType.DMA((z_count + 1,)),
+        ],
+        compiler_params=pltpu.CompilerParams(collective_id=1, has_side_effects=True),
+        name="exchange",
+    )(projected[row_count - longest_window :], docs[row_count - longest_window :], info)
+    return halo, jnp.concatenate([halo_docs, docs]), infos
+
+
+def pool(projected, halo, docs, group_width):
+    row_count, channels = projected.shape
     return pl.pallas_call(
         lambda *refs: pool_kernel(group_width, *refs),
         out_shape=jax.ShapeDtypeStruct((row_count, channels), jnp.bfloat16),
@@ -84,7 +186,7 @@
     return resid, rms_scale(resid, ffn_gain)
 
 
-CHUNKS = 4
+CHUNKS = 8
 
 
 def experts_kernel(
@@ -415,33 +517,25 @@
             to_relay(k, i).wait_send()
 
 
-def run_experts(normed, resid, routes, route_weights, gate, up, down):
+def run_experts(normed, resid, infos, gate, up, down):
     tok, width = normed.shape
     sp_count, tp_count = lax.axis_size("sp"), lax.axis_size("tp")
     x_count = max(tp_count // 2, 1)
     z_count = sp_count // x_count
     plane = x_count * tp_count
-    top_count = routes.shape[1]
+    top_count = infos.shape[1] // 2
     hidden = gate.shape[1]
     capacity = 3 * tok * top_count // (2 * plane * z_count)
     share = -(-z_count * capacity // 16) * 16
-    slots = slots_of(routes, plane * z_count, capacity)
-    info = jnp.concatenate([slots.astype(jnp.float32), route_weights], 1)
     z = lax.axis_index("sp") // x_count
     slot_ids = jnp.arange(plane * share, dtype=jnp.int32)
-    targets, weights = [], []
-    for d in range(z_count):
-        here = info
-        if d:
-            onward = [(s, (s + d * x_count) % sp_count) for s in range(sp_count)]
-            here = lax.ppermute(info, "sp", onward)
-        local = here[:, :top_count].astype(jnp.int32) - z * plane * capacity
-        inside = (local >= 0) & (local < plane * capacity)
-        target = local // capacity * share + d * capacity + local % capacity
-        targets.append(jnp.where(inside, target, -1))
-        weights.append(here[:, top_count:])
-    target, weight = jnp.concatenate(targets), jnp.concatenate(weights)
-    target_t = target.T
+    local = infos[:, :top_count].astype(jnp.int32) - z * plane * capacity
+    inside = (local >= 0) & (local < plane * capacity)
+    base = jnp.arange(z_count, dtype=jnp.int32)[:, None, None] * capacity
+    target = jnp.where(inside, local // capacity * share + base + local % capacity, -1)
+    target_t = target.transpose(1, 0, 2).reshape(top_count, z_count * tok)
+    target = target_t.T
+    weight = infos[:, top_count:].transpose(0, 2, 1).reshape(z_count * tok, top_count)
     select, weigh = False, 0.0
     for j in range(top_count):
         select = select | (slot_ids[:, None] == target_t[j][None, :])
@@ -508,10 +602,11 @@
     expert_up,
     expert_down,
 ):
-    mixed = pool(projected, segments, group_weight.shape[1])
+    halo, docs, infos = exchange(projected, segments, routes, route_weights)
+    mixed = pool(projected, halo, docs, group_weight.shape[1])
     resid, normed = mixer(mixed, stream, group_weight, group_scale, out_weight, ffn_gain)
     return run_experts(
-        normed, resid, routes, route_weights, expert_gate[0], expert_up[0], expert_down[0]
+        normed, resid, infos, expert_gate[0], expert_up[0], expert_down[0]
     )
 
 

time: 174 us -> 177 us (1.017)
  Pallas kernels: 127 us -> 144 us
  starting transfers between devices: 17.3 us -> 3.6 us
    ppermute x5 -> x0, starting transfers between devices: 13.8 us -> none  [the longest x3 6.09 us: run_experts(): here = lax.ppermute(info, 'sp', onward)]
    pallas_call x0 -> x1, Pallas kernels: none -> 9.6 us  [exchange(): pl.pallas_call(lambda *refs: exchange_kernel(z_count, x_count, sp_count,...]
    pallas_call x1, Pallas kernels: 123 us -> 131 us  [run_experts(): pl.pallas_call(lambda *refs: experts_kernel(z_count, x_count, tp_count, *...]
  transfers between devices with their start and end apart: 6 -> 1, of which waited for: 1 -> 1; matrix products, arithmetic and copies ran while one was open for 4% -> 2% of each run, Pallas kernels for 0% -> 0%
where the time goes in v3:
time: 177 us
  Pallas kernels  144 us (81%)
  other arithmetic  9.27 us (5%)
  local copies, waits for them, and re-layouts  8.49 us (5%)
  matrix products  5.97 us (3%)
  waiting for transfers between devices  5.34 us (3%)
  starting transfers between devices  3.6 us (2%)
    pallas_call x1, Pallas kernels, run_experts(): pl.pallas_call(lambda *refs: experts_kernel(z_count, x_count, tp_count, *...  131 us
    pallas_call x1, Pallas kernels, exchange(): pl.pallas_call(lambda *refs: exchange_kernel(z_count, x_count, sp_count,...  9.6 us
    all_to_all x1, waiting for transfers between devices, mixer(): lax.all_to_all(mixed, 'tp', split_axis=0, concat_axis=1, tiled=True)  5.34 us
    dot_general x1, matrix products, mixer(): mixer_out = jnp.dot(scaled, out_weight, preferred_element_type=jnp.float32)  4.84 us
    all_to_all x1, starting transfers between devices, mixer(): lax.all_to_all(mixed, 'tp', split_axis=0, concat_axis=1, tiled=True)  3.6 us
  transfers between devices with their start and end apart: 1, of which 1 were waited for; matrix products, arithmetic and copies ran while one was open for 2% of the time, Pallas kernels for 0%

profile of v3, /device:TPU:0, one launch (start us, length us, event | category | flops | bytes accessed | tf_op | source)
XLA Modules:
  0.0 176.8 jit_solution(16491993879626996092)
XLA Ops:
  0.0 0.8 slice.79
  0.8 0.8 pad.5.clone
  1.5 0.7 convert_reduce_fusion
  2.2 0.1 fusion.27
  2.3 0.7 select_reduce_fusion
  3.1 0.7 add_convert_fusion.1
  3.8 1.3 slice.78.refs_0_
  5.1 1.3 maximum_bitcast_fusion.refs_2_
  6.4 0.7 broadcast_in_dim.77.refs_1_
  7.0 9.6 %exchange.1 = (bf16[16,512]{1,0:T(8,128)(2,1)}, s32[16,128]{1,0:T(8,128)}, f32[4,8,128]{2,1,0:T(8,128)}) custom-call(bf16[16,512]{1,0:T(8,128)(2,1)} %slice.78.refs_0_, s32[16,128]{1,0:T(8,128)} %broadcast_in_dim.77.refs_1_, f32[8,128]{1,0:T(8,128)} %maximum_bitcast_fusion.refs_2_), custom_call_target="tpu_custom_call" | custom-call | tf_op jit(solution)/shard_map/exchange/pallas_call | solution.py:121
  16.6 1.5 pad_add_fusion.refs_2_
  18.2 0.0 copy-start.2
  18.2 3.3 %pool.1 = bf16[512,512]{1,0:T(8,128)(2,1)} custom-call(bf16[16,512]{1,0:T(8,128)(2,1)} %get-tuple-element.8.refs_0_, bf16[512,512]{1,0:T(8,128)(2,1)} %refs_1_.1, s32[528,128]{1,0:T(8,128)} %pad_add_fusion.refs_2_), custom_call_target="tpu_custom_call" | custom-call | tf_op jit(solution)/shard_map/pool/pallas_call | solution.py:145
  21.4 2.0 %copy.18 = bf16[4,128,512]{1,2,0:T(8,128)(2,1)} copy(bf16[4,128,512]{2,1,0:T(8,128)(2,1)} %bitcast.53) | data formatting | bytes 1048576 | tf_op jit(solution)/shard_map/all_to_all | solution.py:170
  23.5 0.0 copy-start
  23.5 3.6 %all-to-all-start = ((bf16[4,128,512]{1,2,0:T(8,128)(2,1)}), bf16[4,128,512]{1,2,0:T(8,128)(2,1)S(1)}, u32[]{:S(2)}, u32[]{:S(2)}) async-start(bf16[4,128,512]{1,2,0:T(8,128)(2,1)} %copy.18), calls=%async_computation | async-start | bytes 1048576 | tf_op jit(solution)/shard_map/all_to_all | solution.py:170
  27.1 0.0 copy-done.2
  27.1 0.1 fusion.38
  27.2 0.1 fusion.39
  27.3 1.5 fusion.4.refs_2_
  28.8 1.7 add_convert_fusion.refs_3_
  30.5 5.3 %all-to-all-done = bf16[4,128,512]{1,2,0:T(8,128)(2,1)S(1)} async-done(((bf16[4,128,512]{1,2,0:T(8,128)(2,1)}), bf16[4,128,512]{1,2,0:T(8,128)(2,1)S(1)}, u32[]{:S(2)}, u32[]{:S(2)}) %all-to-all-start) | async-done | bytes 524320 | tf_op jit(solution)/shard_map/all_to_all | solution.py:170
  35.9 0.0 copy-done
  35.9 0.2 fusion.10
  36.1 0.0 copy-start.4
  36.1 0.0 copy-start.5
  36.1 0.2 fusion.12
  36.4 0.3 fusion.14
  36.7 0.3 fusion.16
  36.9 0.3 copy-done.4
  37.2 0.0 copy-done.5
  37.2 0.0 copy-start.3
  37.2 4.8 %fusion.5 = (f32[128]{0:T(128)S(1)}, bf16[128,2048]{1,0:T(8,128)(2,1)S(1)}) fusion(bf16[2048,2048]{1,0:T(8,128)(2,1)} %param.17, f32[128,512]{1,0:T(8,128)S(1)} %fusion.10, f32[128,512]{1,0:T(8,128)S(1)} %fusion.12, f32[128,512]{1,0:T(8,128)S(1)} %fusion.14, f32[128,512]{1,0:T(8,128)S(1)} %fusion.16, f32[2048]{0:T(1024)S(1)} %copy-done.5, ...), kind=kOutput, calls=%fused_computation.17 | convolution fusion | flops 1076625280 | bytes 10494464 | tf_op jit(solution)/shard_map/dot_general | solution.py:184
  42.0 0.0 copy-start.1
  42.0 0.8 copy-done.1
  42.8 0.0 copy-done.3
  42.8 1.0 fusion.7.refs_0_
  43.8 131.1 %experts.1 = bf16[128,2048]{1,0:T(8,128)(2,1)} custom-call(bf16[128,2048]{1,0:T(8,128)(2,1)} %fusion.7.refs_0_, bf16[128,2048]{1,0:T(8,128)(2,1)} %copy-done.1, bf16[768,512]{1,0:T(8,128)(2,1)} %fusion.4.refs_2_, bf16[512,768]{1,0:T(8,128)(2,1)} %add_convert_fusion.refs_3_, bf16[2048,1024]{1,0:T(8,128)(2,1)} %bitcast.46, bf16[2048,1024]{1,0:T(8,128)(2,1)} %bitcast.47, ...), custom_call_target="tpu_custom_call" | custom-call | tf_op jit(solution)/shard_map/experts/pallas_call | solution.py:552
  174.9 1.9 %copy.20 = bf16[128,2048]{1,0:T(8,128)(2,1)} copy(bf16[128,2048]{1,0:T(8,128)(2,1)} %experts.1) | data formatting | bytes 1048576
  (6 shorter events, 0.0 us)
Async XLA Ops:
  18.2 8.9 %copy-start.2 = (f32[4,8,128]{2,1,0:T(8,128)S(1)}, f32[4,8,128]{2,1,0:T(8,128)}, u32[]{:S(2)}) copy-start(f32[4,8,128]{2,1,0:T(8,128)} %get-tuple-element.10) | copy-start | bytes 49156
  23.5 12.4 %copy-start = (bf16[4,512,512]{2,1,0:T(8,128)(2,1)S(1)}, bf16[4,512,512]{2,1,0:T(8,128)(2,1)}, u32[]{:S(2)}) copy-start(bf16[4,512,512]{2,1,0:T(8,128)(2,1)} %param.15) | copy-start | bytes 6291460
  23.5 12.4 %all-to-all-start = ((bf16[4,128,512]{1,2,0:T(8,128)(2,1)}), bf16[4,128,512]{1,2,0:T(8,128)(2,1)S(1)}, u32[]{:S(2)}, u32[]{:S(2)}) async-start(bf16[4,128,512]{1,2,0:T(8,128)(2,1)} %copy.18), calls=%async_computation | async-start | bytes 1048576 | tf_op jit(solution)/shard_map/all_to_all | solution.py:170
  36.1 1.0 copy-start.4
  36.1 1.0 copy-start.5
  37.2 5.6 %copy-start.3 = (f32[2048]{0:T(1024)S(1)}, f32[2048]{0:T(1024)}, u32[]{:S(2)}) copy-start(f32[2048]{0:T(1024)} %param.18) | copy-start | bytes 24580
  42.0 0.8 copy-start.1
